TPU v7x, 128 devices: a whole 4x4x4 slice. The times are simulated.
128 devices in a mesh: sp: 16 (over z, y), tp: 8 (over x, core).
Axes of the slice: x: 4, y: 4, z: 4, core: 2. Of those that a mesh axis runs over, the one named last changes fastest.
Arguments:
- layer_input_rows: bfloat16 [4096, 2048], P('sp'), may hold values from -6 to 6
- input_norm_gain: float32 [2048], replicated, may hold values from 0.1 to 1.9
- query_weight: bfloat16 [2048, 1024], P(None, 'tp'), may hold values from -0.125 to 0.125
- key_weight: bfloat16 [2048, 1024], P(None, 'tp'), may hold values from -0.125 to 0.125
- value_weight: bfloat16 [2048, 1024], P(None, 'tp'), may hold values from -0.125 to 0.125
- query_norm_gain: float32 [64], replicated, may hold values from 0.5 to 9
- key_norm_gain: float32 [64], replicated, may hold values from 0.5 to 9
- cumulative_gate: float32 [4096, 16], P('sp', 'tp'), may hold values from -575.44 to 0, as said below
- attention_norm_gain: float32 [1024], P('tp'), may hold values from 0.1 to 1.9
- recurrence_query_weight: bfloat16 [2048, 1024], P(None, 'tp'), may hold values from -0.125 to 0.125
- forget_weight: bfloat16 [2048, 1024], P(None, 'tp'), may hold values from -0.125 to 0.125
- recurrence_value_weight: bfloat16 [2048, 1024], P(None, 'tp'), may hold values from -0.125 to 0.125
- output_gate_weight: bfloat16 [2048, 1024], P(None, 'tp'), may hold values from -0.125 to 0.125
- gate_lower_slack: float32 [1024], P('tp'), may hold values from 0 to 0.06
- extra_log_decay: float32 [4096, 8], P('sp', 'tp'), may hold values from -1.5 to 0
- recurrence_norm_gain: float32 [1024], P('tp'), may hold values from 0.1 to 1.9
- attention_output_weight: bfloat16 [1024, 2048], P('tp'), may hold values from -0.125 to 0.125
- recurrence_output_weight: bfloat16 [1024, 2048], P('tp'), may hold values from -0.125 to 0.125
Outputs:
- mixed: bfloat16 [4096, 2048], P(('sp', 'tp'))
- log_sum: float32 [4096, 16], P('sp', 'tp')
Inputs may be any that keep to these rules, and one draw needn't show every extreme that they name: `cumulative_gate`: each column never rises along positions.
All inputs are finite; a program needn't handle non-finite values.
Results may differ from a plain program's by a relative error of at most 0.015.
The roundings to bfloat16 on the way count: a program that leaves them out, or rounds other values in their place, can miss the bound.
Values may be sent and summed in bfloat16 or wider, within the bound.
No kernel may reach another device: no remote copies, remote signals or barrier semaphores. Data moves between devices by JAX's collectives and lax.ppermute only.
A program may use at most 64 MiB of HBM per device.

v0:
```python
import jax
import jax.numpy as jnp
from jax import lax
from jax.experimental import pallas as pl
from jax.experimental.pallas import tpu as pltpu
from jax.sharding import Mesh
from jax.sharding import PartitionSpec as P


HEAD_DIM = 64
EPSILON = 1e-06
ROWS = 256
WIDE = 2048
F32 = jnp.float32
BF16 = jnp.bfloat16
NEG = -1e30
SP = ("z", "y")
TP = ("x", "c")
MISC = 16
K_AT, V_AT, S_AT, M_AT, Y_ROWS = 0, 256, 512, 640, 656
O_S_AT, O_M_AT, Z_ROWS = 256, 384, 400


def dot(a, b, ca=1, cb=0):
    return lax.dot_general(a, b, (((ca,), (cb,)), ((), ())), preferred_element_type=F32)


def lanes(shape):
    return lax.broadcasted_iota(jnp.int32, shape, len(shape) - 1)


def subs(shape):
    return lax.broadcasted_iota(jnp.int32, shape, 0)


def split3(value):
    high = value.astype(BF16)
    rest = value - high.astype(F32)
    middle = rest.astype(BF16)
    low = (rest - middle.astype(F32)).astype(BF16)
    return high, middle, low


def rows_of(value):
    at_lane, at_row = lanes((MISC, 128)), subs((MISC, 128))
    out = None
    for k, part in enumerate(split3(value)):
        pick = ((at_row == k) & (at_lane == 0)) | ((at_row == 3 + k) & (at_lane == 64))
        piece = dot(jnp.where(pick, 1.0, 0.0).astype(BF16), part, 1, 1)
        out = piece if out is None else out + piece
    return out


def packed_rows(rows, extra_high, extra_low):
    first, second = rows[0:8, 0:128], rows[0:8, 128:256]
    at = subs((8, 128))
    first = jnp.where(at == 6, extra_high, jnp.where(at == 7, extra_low, first))
    return jnp.concatenate([first, second], axis=0).astype(BF16)


def spread_rows(misc):
    at_lane, at_row = lanes((MISC, 128)), subs((MISC, 128))
    halves = []
    for base in (0, 8):
        first = (at_row >= base) & (at_row < base + 3) & (at_lane < 64)
        second = (at_row >= base + 3) & (at_row < base + 6) & (at_lane >= 64)
        halves.append(dot(misc, jnp.where(first | second, 1.0, 0.0).astype(BF16), 0, 0))
    return jnp.concatenate(halves, axis=0)


def pair_of(misc):
    return misc[6:7, :].astype(F32) + misc[7:8, :].astype(F32)


def head_norm(value):
    first = lanes(value.shape) < HEAD_DIM
    squares = value * value
    one = jnp.sum(jnp.where(first, squares, 0.0), axis=-1, keepdims=True) / HEAD_DIM
    two = jnp.sum(jnp.where(first, 0.0, squares), axis=-1, keepdims=True) / HEAD_DIM
    return value * jnp.where(first, lax.rsqrt(one + EPSILON), lax.rsqrt(two + EPSILON))


def silu(value):
    return value / (1.0 + jnp.exp(-value))


def project_kernel(
    x_hbm, gain_h, wq_h, wk_h, wv_h, wrq_h, wf_h, wrv_h, wog_h, qg_h, kg_h, cum_h, slack_h, extra_h,
    again_h, rgain_h,
    q_ref, msg_ref, inner_ref, vis_ref, og_ref, cum_out, again_out, rgain_out,
    x_v, wk_v, wv_v, wq_v, wf_v, wrq_v, wrv_v, wog_v,
    gain_ref, qg_ref, kg_ref, cum_ref, slack_ref, extra_ref, again_ref, rgain_ref, sems,
):
    def begin(pairs):
        for src, dst in pairs:
            move = pltpu.make_async_copy(src, dst, sems.at[len(moves)])
            move.start()
            moves.append(move)

    moves = []
    begin([(x_hbm, x_v), (gain_h, gain_ref), (wk_h, wk_v), (wv_h, wv_v)])
    begin([(wq_h, wq_v), (wf_h, wf_v), (wrq_h, wrq_v), (wrv_h, wrv_v), (wog_h, wog_v)])
    begin([(qg_h, qg_ref), (kg_h, kg_ref), (cum_h, cum_ref), (slack_h, slack_ref)])
    begin([(extra_h, extra_ref), (again_h, again_ref), (rgain_h, rgain_ref)])
    moves[0].wait()
    moves[1].wait()
    x = x_v[...].astype(F32)
    mean = jnp.sum(x * x, axis=-1, keepdims=True) / WIDE
    normed = (x * lax.rsqrt(mean + EPSILON) * gain_ref[...]).astype(BF16)

    moves[2].wait()
    moves[3].wait()
    kv = dot(normed, jnp.concatenate([wk_v[...], wv_v[...]], axis=1))
    for move in moves[9:]:
        move.wait()
    cum_out[...] = cum_ref[...]
    again_out[...] = again_ref[...]
    rgain_out[...] = rgain_ref[...]
    kgain = jnp.concatenate([kg_ref[...], kg_ref[...]], axis=1)
    qgain = jnp.concatenate([qg_ref[...], qg_ref[...]], axis=1)
    msg_ref[K_AT:V_AT, :] = (head_norm(kv[:, 0:128]) * kgain).astype(BF16)
    msg_ref[V_AT:S_AT, :] = kv[:, 128:256].astype(BF16)

    moves[4].wait()
    moves[5].wait()
    qf = dot(normed, jnp.concatenate([wq_v[...], wf_v[...]], axis=1))
    query = (head_norm(qf[:, 0:128]) * qgain).astype(BF16)
    q_ref[...] = query * jnp.asarray(HEAD_DIM**-0.5, BF16)
    share = slack_ref[...] / (1.0 + jnp.exp(qf[:, 128:256]))
    log_keep = jnp.log1p(-share)

    moves[6].wait()
    moves[7].wait()
    rr = dot(normed, jnp.concatenate([wrq_v[...], wrv_v[...]], axis=1))
    rec_query = silu(rr[:, 0:128])
    rec_value = rr[:, 128:256].astype(BF16)
    moves[8].wait()
    og_ref[...] = silu(dot(normed, wog_v[...]))

    lower = subs((ROWS, ROWS)) >= lanes((ROWS, ROWS))
    tri = jnp.where(lower, 1.0, 0.0).astype(BF16)
    own_run = None
    for part in split3(log_keep):
        piece = dot(tri, part)
        own_run = piece if own_run is None else own_run + piece
    extra = jnp.where(lower, jnp.broadcast_to(extra_ref[...], (ROWS, ROWS)), 0.0)
    head_col = jnp.broadcast_to(jnp.sum(extra, axis=-1, keepdims=True), (ROWS, ROWS))
    head_run = head_col[:, 0:128]
    head_row = None
    for part in split3(jnp.broadcast_to(extra_ref[...], (MISC, ROWS))):
        piece = dot(part, tri, 1, 1)
        head_row = piece if head_row is None else head_row + piece
    head_row = head_row[0:1, :]
    fading = jnp.exp(jnp.where(lower, head_col - head_row, NEG))
    left = (rec_query * jnp.exp(own_run)).astype(BF16)
    right = (share * jnp.exp(-own_run)).astype(BF16)
    scores = (dot(left, right, 1, 1) * fading).astype(BF16)
    inner_ref[...] = dot(scores, rec_value)
    run = own_run + head_run
    closing = run[ROWS - 1 : ROWS, :]
    vis_ref[...] = (rec_query * jnp.exp(run)).astype(BF16)
    into = (share * jnp.exp(closing - run)).astype(BF16)
    msg_ref[S_AT:M_AT, :] = dot(rec_value, into, 0, 0).astype(BF16)
    parts = [p.astype(F32) for p in split3(-cum_ref[...])]
    rows = [p[0:1, :] for p in parts] + [p[1:2, :] for p in parts]
    rows = jnp.concatenate(rows + [jnp.zeros((2, ROWS), F32)], axis=0)
    high, middle, _ = split3(closing)
    msg_ref[M_AT:Y_ROWS, :] = packed_rows(rows, high.astype(F32), middle.astype(F32))


def spread_keys(misc, head):
    at_lane, at_row = lanes((MISC, 128)), subs((MISC, 128))
    start = HEAD_DIM * (1 - head)
    halves = []
    for base in (3 * head, 8 + 3 * head):
        pick = (at_lane - start == at_row - base) & (at_row >= base) & (at_row < base + 3)
        halves.append(dot(misc, jnp.where(pick, 1.0, 0.0).astype(BF16), 0, 0))
    return jnp.concatenate(halves, axis=0).astype(BF16)


def key_sides(msgs):
    first = lanes((ROWS, 128)) < HEAD_DIM
    keys = []
    for head in (0, 1):
        mine = first if head == 0 else ~first
        keys.append(
            jnp.concatenate(
                [jnp.where(mine, m[K_AT:V_AT, :], spread_keys(m[M_AT:Y_ROWS, :], head)) for m in msgs],
                axis=0,
            )
        )
    values = jnp.concatenate([m[V_AT:S_AT, :] for m in msgs], axis=0)
    return keys, jnp.concatenate([values, jnp.ones_like(values)], axis=1)


def attend(query, keys, values, masks):
    at = lanes((128, 128))
    first = at < HEAD_DIM
    one, zero = jnp.ones((128, 128), BF16), jnp.zeros((128, 128), BF16)
    chains = [(row, head) for row in range(0, ROWS, 128) for head in (0, 1)]
    scores, results = {}, {}

    def score(row, head):
        start = HEAD_DIM * (1 - head)
        other = jnp.where((at >= start) & (at < start + 3), one, zero)
        mine = jnp.where(first if head == 0 else ~first, query[row : row + 128, :], other)
        found = dot(mine, keys[head], 1, 1)
        if masks is not None:
            found = jnp.where(masks[row : row + 128, :], found, NEG)
        return found

    def finish(found):
        top = jnp.max(found, axis=-1, keepdims=True)
        summed = dot(jnp.exp(found - top).astype(BF16), values)
        totals = summed[:, 128:256]
        return summed[:, 0:128] / totals, top + jnp.log(totals)

    for chain in chains:
        scores[chain] = score(*chain)
    for chain in chains:
        results[chain] = finish(scores[chain])
    return tuple(
        jnp.concatenate(
            [
                jnp.where(first, results[row, 0][k], results[row, 1][k])
                for row in range(0, ROWS, 128)
            ],
            axis=0,
        )
        for k in (0, 1)
    )


def places(y):
    return [lax.rem(y - o + 4, 4) for o in range(4)]


def remote_kernel(at_ref, m0, m1, m2, m3, q1, q2, q3, o1, o2, o3, keys_ref, values_ref):
    z, y = at_ref[0], at_ref[1]
    msgs = (m0, m1, m2, m3)
    where = places(y)
    decays = [pair_of(m[M_AT:Y_ROWS, :]) for m in msgs]
    state = jnp.zeros((128, 128), F32)
    for a in range(4):
        after = jnp.zeros((1, 128), F32)
        for b in range(4):
            if b != a:
                after = after + jnp.where(where[b] > where[a], decays[b], 0.0)
        state = state + msgs[a][S_AT:M_AT, :].astype(F32) * jnp.exp(after)
    state = state.astype(BF16)
    high, middle, _ = split3(decays[0] + decays[1] + decays[2] + decays[3])

    @pl.when(z < 3)
    def _():
        keys, values = key_sides(msgs)
        keys_ref[0], keys_ref[1] = keys
        values_ref[...] = values

    for o, (query, out) in enumerate(((q1, o1), (q2, o2), (q3, o3)), 1):

        @pl.when(z + o < 4)
        def _(query=query, out=out):
            result, log_total = attend(query[...], (keys_ref[0], keys_ref[1]), values_ref[...], None)
            out[0:O_S_AT, :] = result.astype(BF16)
            out[O_S_AT:O_M_AT, :] = state
            out[O_M_AT:Z_ROWS, :] = packed_rows(
                rows_of(log_total), high.astype(F32), middle.astype(F32)
            )


def local_kernel(at_ref, q_ref, m0, m1, m2, m3, inner_ref, vis_ref, o_ref, lse_ref, rec_ref, before_ref):
    y = at_ref[1]
    msgs = (m0, m1, m2, m3)
    where = places(y)
    decays = [pair_of(m[M_AT:Y_ROWS, :]) for m in msgs]
    state = jnp.zeros((128, 128), F32)
    whole = jnp.zeros((1, 128), F32)
    for a in range(1, 4):
        between = jnp.zeros((1, 128), F32)
        for b in range(1, 4):
            if b != a:
                seen = (where[b] > where[a]) & (where[b] < y)
                between = between + jnp.where(seen, decays[b], 0.0)
        piece = msgs[a][S_AT:M_AT, :].astype(F32) * jnp.exp(between)
        state = state + jnp.where(where[a] < y, piece, 0.0)
        whole = whole + jnp.where(where[a] < y, decays[a], 0.0)
    before_ref[...] = jnp.broadcast_to(jnp.exp(whole), (8, 128))
    rec_ref[...] = inner_ref[...] + dot(vis_ref[...], state.astype(BF16), 1, 1)
    shape = (ROWS, 4 * ROWS)
    at = lanes(shape)
    earlier = subs(shape) >= at
    full = jnp.where(y >= 1, 512, 256)
    full = jnp.where(y >= 2, 768, full)
    full = jnp.where(y >= 3, 1024, full)
    masks = earlier | ((at >= 256) & (at < full))
    result, log_total = attend(q_ref[...], *key_sides(msgs), masks)
    o_ref[...] = result
    lse_ref[...] = log_total


def join_kernel(
    at_ref, o_ref, lse_ref, rec_ref, before_ref, vis_ref, og_ref, again_ref, rgain_ref, r1, r2, r3,
    keep_ref, give_ref, log_ref, both_ref,
):
    z, c = at_ref[0], at_ref[2]
    got = (r1, r2, r3)
    lses = [lse_ref[...]]
    outs = [o_ref[...]]
    for o, r in enumerate(got, 1):
        lses.append(jnp.where(z >= o, spread_rows(r[O_M_AT:Z_ROWS, :]), NEG))
        outs.append(r[0:O_S_AT, :].astype(F32))
    top = jnp.maximum(jnp.maximum(lses[0], lses[1]), jnp.maximum(lses[2], lses[3]))
    total, summed = 0.0, 0.0
    for value, out in zip(lses, outs):
        weight = jnp.exp(value - top)
        total = total + weight
        summed = summed + weight * out
    log_ref[...] = top + jnp.log(total)
    both_ref[:, 0:128] = (head_norm(summed / total) * again_ref[...]).astype(BF16)

    decays = [pair_of(r[O_M_AT:Z_ROWS, :]) for r in got]
    state = r1[O_S_AT:O_M_AT, :].astype(F32)
    state = state + r2[O_S_AT:O_M_AT, :].astype(F32) * jnp.exp(decays[0])
    state = state + r3[O_S_AT:O_M_AT, :].astype(F32) * jnp.exp(decays[0] + decays[1])
    state = (state * before_ref[0:1, :]).astype(BF16)
    rec = rec_ref[...] + dot(vis_ref[...], state, 1, 1)
    mean = jnp.sum(rec * rec, axis=-1, keepdims=True) / 128
    rec = rec * lax.rsqrt(mean + EPSILON) * rgain_ref[...] * og_ref[...]
    both_ref[:, 128:256] = rec.astype(BF16)
    for k in range(4):
        keep_ref[32 * k : 32 * k + 32, :] = both_ref[pl.ds(64 * k + 32 * c, 32), :]
        give_ref[32 * k : 32 * k + 32, :] = both_ref[pl.ds(64 * k + 32 * (1 - c), 32), :]


def log_kernel(total_ref, cum_ref, log_ref):
    rows = rows_of(total_ref[...])
    log_ref[0:1, :] = rows[0:1, :] + rows[1:2, :] + rows[2:3, :] + cum_ref[0:1, :]
    log_ref[1:2, :] = rows[3:4, :] + rows[4:5, :] + rows[5:6, :] + cum_ref[1:2, :]


def out_kernel(at_ref, keep_ref, got_ref, wa, wr, pa, pr, s0, s1, s2, s3, sum_ref):
    x = at_ref[3]
    both = jnp.concatenate([keep_ref[...], got_ref[...]], axis=1)
    for k in range(4):
        cols = slice(512 * k, 512 * k + 512)
        weight = jnp.concatenate([wa[:, cols], wr[:, cols], pa[:, cols], pr[:, cols]], axis=0)
        sum_ref[:, cols] = dot(both, weight).astype(BF16)
    for o, out in enumerate((s0, s1, s2, s3)):
        out[...] = sum_ref[pl.ds(32 * lax.rem(x + o, 4), 32), :]


def add_kernel(a, b, c, d, out):
    out[...] = (
        (a[...].astype(F32) + b[...].astype(F32)) + (c[...].astype(F32) + d[...].astype(F32))
    ).astype(BF16)


VM = pl.BlockSpec(memory_space=pltpu.VMEM)
SM = pl.BlockSpec(memory_space=pltpu.SMEM)
ANY = pl.BlockSpec(memory_space=pltpu.HBM)


def call(kernel, specs, shapes, scratch=()):
    return pl.pallas_call(
        kernel,
        in_specs=specs,
        out_specs=[VM] * len(shapes),
        out_shape=[jax.ShapeDtypeStruct(s, d) for s, d in shapes],
        scratch_shapes=list(scratch),
        compiler_params=pltpu.CompilerParams(vmem_limit_bytes=32 * 1024 * 1024),
    )


def far(value):
    return pltpu.with_memory_space_constraint(value, pltpu.HBM)


def turned(value, axis, by):
    return lax.ppermute(value, axis, [(i, (i + by) % 4) for i in range(4)])


def moved(value, axis, by):
    return lax.ppermute(value, axis, [(i, i + by) for i in range(4) if 0 <= i + by < 4])


def body(
    layer_input_rows, input_norm_gain, query_weight, key_weight, value_weight, query_norm_gain,
    key_norm_gain, cumulative_gate, attention_norm_gain, recurrence_query_weight, forget_weight,
    recurrence_value_weight, output_gate_weight, gate_lower_slack, extra_log_decay,
    recurrence_norm_gain, attention_output_weight, recurrence_output_weight,
):
    z, y, x, c = (lax.axis_index(a) for a in ("z", "y", "x", "c"))
    at = jnp.stack([z, y, c, x]).astype(jnp.int32)
    swap = [(0, 1), (1, 0)]
    gate_rows = cumulative_gate.T
    w = pltpu.VMEM((WIDE, 128), BF16)
    tall = (ROWS, 128)
    query, msg, inner, vis, gate, gate_near, again, rgain = call(
        project_kernel,
        [ANY] * 16,
        [(tall, BF16), ((Y_ROWS, 128), BF16), (tall, F32), (tall, BF16), (tall, F32),
         ((2, ROWS), F32), ((1, 128), F32), ((1, 128), F32)],
        [pltpu.VMEM((ROWS, WIDE), BF16)] + [w] * 7
        + [pltpu.VMEM(n, F32) for n in ((1, WIDE), (1, 64), (1, 64), (2, ROWS), (1, 128), (1, ROWS), (1, 128), (1, 128))]
        + [pltpu.SemaphoreType.DMA((16,))],
    )(
        *[
            far(value)
            for value in (
                layer_input_rows, input_norm_gain.reshape(1, WIDE), query_weight, key_weight,
                value_weight, recurrence_query_weight, forget_weight, recurrence_value_weight,
                output_gate_weight, query_norm_gain.reshape(1, 64), key_norm_gain.reshape(1, 64),
                gate_rows, gate_lower_slack.reshape(1, 128), extra_log_decay.T,
                attention_norm_gain.reshape(1, 128), recurrence_norm_gain.reshape(1, 128),
            )
        ]
    )
    msgs = [msg] + [turned(msg, "y", o) for o in (1, 2, 3)]
    queries = [moved(query, "z", -o) for o in (1, 2, 3)]
    wa, wr, _ = lax.optimization_barrier((attention_output_weight, recurrence_output_weight, query))
    pa = lax.ppermute(wa, "c", swap)
    pr = lax.ppermute(wr, "c", swap)
    sent = call(
        remote_kernel, [SM] + [VM] * 7, [((Z_ROWS, 128), BF16)] * 3,
        [pltpu.VMEM((2, 4 * ROWS, 128), BF16), pltpu.VMEM((4 * ROWS, 256), BF16)],
    )(at, *msgs, *queries)
    got = [moved(s, "z", o) for o, s in enumerate(sent, 1)]
    out, lse, rec, before = call(
        local_kernel, [SM] + [VM] * 7, [(tall, F32), (tall, F32), (tall, F32), ((8, 128), F32)]
    )(at, query, *msgs, inner, vis)
    keep, give, log_total = call(
        join_kernel,
        [SM] + [VM] * 11,
        [((128, 256), BF16), ((128, 256), BF16), (tall, F32)],
        [pltpu.VMEM((ROWS, 256), BF16)],
    )(
        at, out, lse, rec, before, vis, gate, again, rgain, *got,
    )
    log_sum = call(log_kernel, [VM] * 2, [((2, ROWS), F32)])(log_total, gate_near)[0]
    taken = lax.ppermute(give, "c", swap)
    shares = call(
        out_kernel, [SM] + [VM] * 6, [((32, WIDE), BF16)] * 4, [pltpu.VMEM((128, WIDE), BF16)]
    )(at, keep, taken, attention_output_weight, recurrence_output_weight, pa, pr)
    arrived = [shares[0]] + [turned(shares[o], "x", o) for o in (1, 2, 3)]
    mixed = call(add_kernel, [VM] * 4, [((32, WIDE), BF16)])(*arrived)[0]
    return (mixed, log_sum.T)


def solution(mesh):
    finer = Mesh(mesh.devices.reshape(4, 4, 4, 2), ("z", "y", "x", "c"))
    column = P(None, TP)
    placed = (
        P(SP, None), P(), column, column, column, P(), P(), P(SP, TP), P(TP), column, column,
        column, column, P(TP), P(SP, TP), P(TP), P(TP, None), P(TP, None),
    )
    return jax.shard_map(
        body, mesh=finer, in_specs=placed, out_specs=(P(SP + TP, None), P(SP, TP)), check_vma=False
    )
```

profile of v0, /device:TPU:1, one launch (start us, length us, event | category | flops | bytes accessed | tf_op | source)
XLA Modules:
  0.0 54.0 jit_solution(1670285108322851300)
XLA Ops:
  0.7 5.3 %shard_map.185 = (bf16[256,128]{1,0:T(8,128)(2,1)S(1)}, bf16[656,128]{1,0:T(8,128)(2,1)S(1)}, f32[256,128]{1,0:T(8,128)S(1)}, bf16[256,128]{1,0:T(8,128)(2,1)S(1...) custom-call(bf16[256,2048]{1,0:T(8,128)(2,1)} %x_hbm.1, ...), custom_call_target="tpu_custom_call" | custom-call | tf_op jit(solution)/shard_map/pallas_call | solution.py:398
  6.0 1.5 %collective-permute-start.10 = (bf16[128,2048]{1,0:T(8,128)(2,1)S(1)}, bf16[128,2048]{1,0:T(8,128)(2,1)S(1)}, u32[]{:S(2)}, u32[]{:S(2)}) collective-permute-start(bf16[128,2048]{1,0:T(8,128)(2,1)S(1)} %copy-done), channel_id=1, source_target_pairs={{0,1},{1,0},{2,3},{3,2},{4,5},{5,4},{6,7},{7,6},{8,9},{9,8},{10,11... | collective-permute-start | bytes 1572872 | tf_op jit(solution)/shard_map/ppermute | solution.py:421
  7.5 0.1 collective-permute-start.11
  7.6 1.3 %collective-permute-start.5 = (bf16[256,128]{1,0:T(8,128)(2,1)S(1)}, bf16[256,128]{1,0:T(8,128)(2,1)S(1)}, u32[]{:S(2)}, u32[]{:S(2)}) collective-permute-start(bf16[256,128]{1,0:T(8,128)(2,1)S(1)} %get-tuple-element.26.q_ref), channel_id=1, source_target_pairs={{96,0},{97,1},{98,2},{99,3},{100,4},{101,5},{102,6},{103,7},{104,8... | collective-permute-start | bytes 196616 | tf_op jit(solution)/shard_map/ppermute | solution.py:383
  8.9 1.3 %collective-permute-start.4 = (bf16[256,128]{1,0:T(8,128)(2,1)S(1)}, bf16[256,128]{1,0:T(8,128)(2,1)S(1)}, u32[]{:S(2)}, u32[]{:S(2)}) collective-permute-start(bf16[256,128]{1,0:T(8,128)(2,1)S(1)} %get-tuple-element.26.q_ref), channel_id=1, source_target_pairs={{64,0},{96,32},{65,1},{97,33},{66,2},{98,34},{67,3},{99,35},{68,4}... | collective-permute-start | bytes 196616 | tf_op jit(solution)/shard_map/ppermute | solution.py:383
  10.2 1.3 %collective-permute-start.3 = (bf16[256,128]{1,0:T(8,128)(2,1)S(1)}, bf16[256,128]{1,0:T(8,128)(2,1)S(1)}, u32[]{:S(2)}, u32[]{:S(2)}) collective-permute-start(bf16[256,128]{1,0:T(8,128)(2,1)S(1)} %get-tuple-element.26.q_ref), channel_id=1, source_target_pairs={{32,0},{64,32},{96,64},{33,1},{65,33},{97,65},{34,2},{66,34},{98,6... | collective-permute-start | bytes 196616 | tf_op jit(solution)/shard_map/ppermute | solution.py:383
  11.5 3.3 %collective-permute-done.5.q3 = bf16[256,128]{1,0:T(8,128)(2,1)S(1)} collective-permute-done((bf16[256,128]{1,0:T(8,128)(2,1)S(1)}, bf16[256,128]{1,0:T(8,128)(2,1)S(1)}, u32[]{:S(2)}, u32[]{:S(2)}) %collective-permute-start.5) | collective-permute-done | bytes 65568 | tf_op jit(solution)/shard_map/ppermute | solution.py:383
  14.8 2.7 %collective-permute-start.2 = (bf16[656,128]{1,0:T(8,128)(2,1)S(1)}, bf16[656,128]{1,0:T(8,128)(2,1)S(1)}, u32[]{:S(2)}, u32[]{:S(2)}) collective-permute-start(bf16[656,128]{1,0:T(8,128)(2,1)S(1)} %get-tuple-element.27.m0), channel_id=1, source_target_pairs={{0,24},{8,0},{16,8},{24,16},{1,25},{9,1},{17,9},{25,17},{2,26},{10... | collective-permute-start | bytes 503816 | tf_op jit(solution)/shard_map/ppermute | solution.py:379
  17.5 0.0 collective-permute-done.4.q2
  17.5 1.0 %collective-permute-start.1 = (bf16[656,128]{1,0:T(8,128)(2,1)S(1)}, bf16[656,128]{1,0:T(8,128)(2,1)S(1)}, u32[]{:S(2)}, u32[]{:S(2)}) collective-permute-start(bf16[656,128]{1,0:T(8,128)(2,1)S(1)} %get-tuple-element.27.m0), channel_id=1, source_target_pairs={{0,16},{8,24},{16,0},{24,8},{1,17},{9,25},{17,1},{25,9},{2,18},{10... | collective-permute-start | bytes 503816 | tf_op jit(solution)/shard_map/ppermute | solution.py:379
  18.5 0.0 collective-permute-done.3.q1
  18.5 0.4 collective-permute-start
  18.9 0.1 pad_add_fusion.at_ref
  19.0 1.5 %collective-permute-done.2.m3 = bf16[656,128]{1,0:T(8,128)(2,1)S(1)} collective-permute-done((bf16[656,128]{1,0:T(8,128)(2,1)S(1)}, bf16[656,128]{1,0:T(8,128)(2,1)S(1)}, u32[]{:S(2)}, u32[]{:S(2)}) %collective-permute-start.2) | collective-permute-done | bytes 167968 | tf_op jit(solution)/shard_map/ppermute | solution.py:379
  20.5 2.8 %collective-permute-done.1.m2 = bf16[656,128]{1,0:T(8,128)(2,1)S(1)} collective-permute-done((bf16[656,128]{1,0:T(8,128)(2,1)S(1)}, bf16[656,128]{1,0:T(8,128)(2,1)S(1)}, u32[]{:S(2)}, u32[]{:S(2)}) %collective-permute-start.1) | collective-permute-done | bytes 167968 | tf_op jit(solution)/shard_map/ppermute | solution.py:379
  23.3 4.1 %collective-permute-done.m1 = bf16[656,128]{1,0:T(8,128)(2,1)S(1)} collective-permute-done((bf16[656,128]{1,0:T(8,128)(2,1)S(1)}, bf16[656,128]{1,0:T(8,128)(2,1)S(1)}, u32[]{:S(2)}, u32[]{:S(2)}) %collective-permute-start) | collective-permute-done | bytes 167968 | tf_op jit(solution)/shard_map/ppermute | solution.py:379
  27.4 4.2 %shard_map.187 = (bf16[400,128]{1,0:T(8,128)(2,1)S(1)}, bf16[400,128]{1,0:T(8,128)(2,1)S(1)}, bf16[400,128]{1,0:T(8,128)(2,1)S(1)}) custom-call(s32[4]{0:T(128)S(1)} %pad_add_fusion.at_ref, bf16[656,128]{1,0:T(8,128)(2,1)S(1)} %get-tuple-element.27.m0, bf16[656,128]{1,0:T(8,128)(2,1)S(1)} %collective-permute-done.m1, ...), custom_call_target="tpu_custom_call" | custom-call | tf_op jit(solution)/shard_map/pallas_call | solution.py:423
  31.6 1.3 %collective-permute-start.6 = (bf16[400,128]{1,0:T(8,128)(2,1)S(1)}, bf16[400,128]{1,0:T(8,128)(2,1)S(1)}, u32[]{:S(2)}, u32[]{:S(2)}) collective-permute-start(bf16[400,128]{1,0:T(8,128)(2,1)S(1)} %get-tuple-element.37), channel_id=1, source_target_pairs={{0,32},{32,64},{64,96},{1,33},{33,65},{65,97},{2,34},{34,66},{66,9... | collective-permute-start | bytes 307208 | tf_op jit(solution)/shard_map/ppermute | solution.py:383
  32.9 2.9 %collective-permute-start.7 = (bf16[400,128]{1,0:T(8,128)(2,1)S(1)}, bf16[400,128]{1,0:T(8,128)(2,1)S(1)}, u32[]{:S(2)}, u32[]{:S(2)}) collective-permute-start(bf16[400,128]{1,0:T(8,128)(2,1)S(1)} %get-tuple-element.38), channel_id=1, source_target_pairs={{0,64},{32,96},{1,65},{33,97},{2,66},{34,98},{3,67},{35,99},{4,68}... | collective-permute-start | bytes 307208 | tf_op jit(solution)/shard_map/ppermute | solution.py:383
  35.8 1.3 %collective-permute-start.8 = (bf16[400,128]{1,0:T(8,128)(2,1)S(1)}, bf16[400,128]{1,0:T(8,128)(2,1)S(1)}, u32[]{:S(2)}, u32[]{:S(2)}) collective-permute-start(bf16[400,128]{1,0:T(8,128)(2,1)S(1)} %get-tuple-element.39), channel_id=1, source_target_pairs={{0,96},{1,97},{2,98},{3,99},{4,100},{5,101},{6,102},{7,103},{8,104... | collective-permute-start | bytes 307208 | tf_op jit(solution)/shard_map/ppermute | solution.py:383
  37.1 1.7 %shard_map.186 = (f32[256,128]{1,0:T(8,128)S(1)}, f32[256,128]{1,0:T(8,128)S(1)}, f32[256,128]{1,0:T(8,128)S(1)}, f32[8,128]{1,0:T(8,128)S(1)}) custom-call(s32[4]{0:T(128)S(1)} %pad_add_fusion.at_ref, bf16[256,128]{1,0:T(8,128)(2,1)S(1)} %get-tuple-element.26.q_ref, bf16[656,128]{1,0:T(8,128)(2,1)S(1)} %get-tuple-element.27.m0, ...), custom_call_target="tpu_custom_call" | custom-call | tf_op jit(solution)/shard_map/pallas_call | solution.py:428
  38.9 1.1 %shard_map.188 = (bf16[128,256]{1,0:T(8,128)(2,1)S(1)}, bf16[128,256]{1,0:T(8,128)(2,1)S(1)}, f32[256,128]{1,0:T(8,128)S(1)}) custom-call(s32[4]{0:T(128)S(1)} %pad_add_fusion.at_ref, f32[256,128]{1,0:T(8,128)S(1)} %get-tuple-element.30.o_ref, f32[256,128]{1,0:T(8,128)S(1)} %get-tuple-element.31.lse_ref, f32[256,128]{1,0:T(8,128)S(1)} %get-tuple-element.32.rec_ref, ...), custom_call_target="tpu_custom_call" | custom-call | tf_op jit(solution)/shard_map/pallas_call | solution.py:431
  39.9 1.6 %collective-permute-start.9 = (bf16[128,256]{1,0:T(8,128)(2,1)S(1)}, bf16[128,256]{1,0:T(8,128)(2,1)S(1)}, u32[]{:S(2)}, u32[]{:S(2)}) collective-permute-start(bf16[128,256]{1,0:T(8,128)(2,1)S(1)} %get-tuple-element.41), channel_id=1, source_target_pairs={{0,1},{1,0},{2,3},{3,2},{4,5},{5,4},{6,7},{7,6},{8,9},{9,8},{10,11... | collective-permute-start | bytes 196616 | tf_op jit(solution)/shard_map/ppermute | solution.py:440
  41.5 0.9 %collective-permute-done.9.got_ref = bf16[128,256]{1,0:T(8,128)(2,1)S(1)} collective-permute-done((bf16[128,256]{1,0:T(8,128)(2,1)S(1)}, bf16[128,256]{1,0:T(8,128)(2,1)S(1)}, u32[]{:S(2)}, u32[]{:S(2)}) %collective-permute-start.9) | collective-permute-done | bytes 65568 | tf_op jit(solution)/shard_map/ppermute | solution.py:440
  42.4 1.0 %shard_map.189 = (bf16[32,2048]{1,0:T(8,128)(2,1)S(1)}, bf16[32,2048]{1,0:T(8,128)(2,1)S(1)}, bf16[32,2048]{1,0:T(8,128)(2,1)S(1)}, bf16[32,2048]{1,0:T(8,128)(2,1)S(1)}) custom-call(s32[4]{0:T(128)S(1)} %pad_add_fusion.at_ref, bf16[128,256]{1,0:T(8,128)(2,1)S(1)} %get-tuple-element.40.keep_ref, bf16[128,256]{1,0:T(8,128)(2,1)S(1)} %collective-permute-done.9.got_ref, ...), custom_call_target="tpu_custom_call" | custom-call | tf_op jit(solution)/shard_map/pallas_call | solution.py:441
  43.5 1.3 %collective-permute-start.12 = (bf16[32,2048]{1,0:T(8,128)(2,1)S(1)}, bf16[32,2048]{1,0:T(8,128)(2,1)S(1)}, u32[]{:S(2)}, u32[]{:S(2)}) collective-permute-start(bf16[32,2048]{1,0:T(8,128)(2,1)S(1)} %get-tuple-element.45), channel_id=1, source_target_pairs={{0,2},{2,4},{4,6},{6,0},{1,3},{3,5},{5,7},{7,1},{8,10},{10,12},{12... | collective-permute-start | bytes 393224 | tf_op jit(solution)/shard_map/ppermute | solution.py:379
  44.8 2.4 %collective-permute-start.13 = (bf16[32,2048]{1,0:T(8,128)(2,1)S(1)}, bf16[32,2048]{1,0:T(8,128)(2,1)S(1)}, u32[]{:S(2)}, u32[]{:S(2)}) collective-permute-start(bf16[32,2048]{1,0:T(8,128)(2,1)S(1)} %get-tuple-element.46), channel_id=1, source_target_pairs={{0,4},{2,6},{4,0},{6,2},{1,5},{3,7},{5,1},{7,3},{8,12},{10,14},{12... | collective-permute-start | bytes 393224 | tf_op jit(solution)/shard_map/ppermute | solution.py:379
  47.2 1.2 %collective-permute-start.14 = (bf16[32,2048]{1,0:T(8,128)(2,1)S(1)}, bf16[32,2048]{1,0:T(8,128)(2,1)S(1)}, u32[]{:S(2)}, u32[]{:S(2)}) collective-permute-start(bf16[32,2048]{1,0:T(8,128)(2,1)S(1)} %get-tuple-element.47), channel_id=1, source_target_pairs={{0,6},{2,0},{4,2},{6,4},{1,7},{3,1},{5,3},{7,5},{8,14},{10,8},{12,... | collective-permute-start | bytes 393224 | tf_op jit(solution)/shard_map/ppermute | solution.py:379
  48.4 0.8 %shard_map.191 = f32[2,256]{1,0:T(2,128)} custom-call(f32[256,128]{1,0:T(8,128)S(1)} %get-tuple-element.48.total_ref, f32[2,256]{1,0:T(2,128)S(1)} %get-tuple-element.49.cum_ref), custom_call_target="tpu_custom_call" | custom-call | tf_op jit(solution)/shard_map/pallas_call | solution.py:439
  49.1 0.3 collective-permute-done.12.b
  49.5 3.8 %collective-permute-done.13.c = bf16[32,2048]{1,0:T(8,128)(2,1)S(1)} collective-permute-done((bf16[32,2048]{1,0:T(8,128)(2,1)S(1)}, bf16[32,2048]{1,0:T(8,128)(2,1)S(1)}, u32[]{:S(2)}, u32[]{:S(2)}) %collective-permute-start.13) | collective-permute-done | bytes 131104 | tf_op jit(solution)/shard_map/ppermute | solution.py:379
  53.3 0.7 %shard_map.190 = bf16[32,2048]{1,0:T(8,128)(2,1)} custom-call(bf16[32,2048]{1,0:T(8,128)(2,1)S(1)} %get-tuple-element.44.a, bf16[32,2048]{1,0:T(8,128)(2,1)S(1)} %collective-permute-done.12.b, bf16[32,2048]{1,0:T(8,128)(2,1)S(1)} %collective-permute-done.13.c, bf16[32,2048]{1,0:T(8,128)(2,1)S(1)} %collective-permute-done.14.d), custom_call_target="tpu_custom_call" | custom-call | tf_op jit(solution)/shard_map/pallas_call | solution.py:445
  (10 shorter events, 0.0 us)
Async XLA Ops:
  0.6 5.4 %copy-start = (bf16[128,2048]{1,0:T(8,128)(2,1)S(1)}, bf16[128,2048]{1,0:T(8,128)(2,1)}, u32[]{:S(2)}) copy-start(bf16[128,2048]{1,0:T(8,128)(2,1)} %wa.1) | copy-start | bytes 1572868
  0.6 6.8 %copy-start.1 = (bf16[128,2048]{1,0:T(8,128)(2,1)S(1)}, bf16[128,2048]{1,0:T(8,128)(2,1)}, u32[]{:S(2)}) copy-start(bf16[128,2048]{1,0:T(8,128)(2,1)} %wr.1) | copy-start | bytes 1572868
  6.0 36.4 %collective-permute-start.10 = (bf16[128,2048]{1,0:T(8,128)(2,1)S(1)}, bf16[128,2048]{1,0:T(8,128)(2,1)S(1)}, u32[]{:S(2)}, u32[]{:S(2)}) collective-permute-start(bf16[128,2048]{1,0:T(8,128)(2,1)S(1)} %copy-done), channel_id=1, source_target_pairs={{0,1},{1,0},{2,3},{3,2},{4,5},{5,4},{6,7},{7,6},{8,9},{9,8},{10,11... | collective-permute-start | bytes 1572872 | tf_op jit(solution)/shard_map/ppermute | solution.py:421
  7.5 35.0 %collective-permute-start.11 = (bf16[128,2048]{1,0:T(8,128)(2,1)S(1)}, bf16[128,2048]{1,0:T(8,128)(2,1)S(1)}, u32[]{:S(2)}, u32[]{:S(2)}) collective-permute-start(bf16[128,2048]{1,0:T(8,128)(2,1)S(1)} %copy-done.1), channel_id=1, source_target_pairs={{0,1},{1,0},{2,3},{3,2},{4,5},{5,4},{6,7},{7,6},{8,9},{9,8},{10,11... | collective-permute-start | bytes 1572872 | tf_op jit(solution)/shard_map/ppermute | solution.py:422
  7.6 7.2 %collective-permute-start.5 = (bf16[256,128]{1,0:T(8,128)(2,1)S(1)}, bf16[256,128]{1,0:T(8,128)(2,1)S(1)}, u32[]{:S(2)}, u32[]{:S(2)}) collective-permute-start(bf16[256,128]{1,0:T(8,128)(2,1)S(1)} %get-tuple-element.26.q_ref), channel_id=1, source_target_pairs={{96,0},{97,1},{98,2},{99,3},{100,4},{101,5},{102,6},{103,7},{104,8... | collective-permute-start | bytes 196616 | tf_op jit(solution)/shard_map/ppermute | solution.py:383
  8.9 8.6 %collective-permute-start.4 = (bf16[256,128]{1,0:T(8,128)(2,1)S(1)}, bf16[256,128]{1,0:T(8,128)(2,1)S(1)}, u32[]{:S(2)}, u32[]{:S(2)}) collective-permute-start(bf16[256,128]{1,0:T(8,128)(2,1)S(1)} %get-tuple-element.26.q_ref), channel_id=1, source_target_pairs={{64,0},{96,32},{65,1},{97,33},{66,2},{98,34},{67,3},{99,35},{68,4}... | collective-permute-start | bytes 196616 | tf_op jit(solution)/shard_map/ppermute | solution.py:383
  10.2 8.3 %collective-permute-start.3 = (bf16[256,128]{1,0:T(8,128)(2,1)S(1)}, bf16[256,128]{1,0:T(8,128)(2,1)S(1)}, u32[]{:S(2)}, u32[]{:S(2)}) collective-permute-start(bf16[256,128]{1,0:T(8,128)(2,1)S(1)} %get-tuple-element.26.q_ref), channel_id=1, source_target_pairs={{32,0},{64,32},{96,64},{33,1},{65,33},{97,65},{34,2},{66,34},{98,6... | collective-permute-start | bytes 196616 | tf_op jit(solution)/shard_map/ppermute | solution.py:383
  14.8 5.8 %collective-permute-start.2 = (bf16[656,128]{1,0:T(8,128)(2,1)S(1)}, bf16[656,128]{1,0:T(8,128)(2,1)S(1)}, u32[]{:S(2)}, u32[]{:S(2)}) collective-permute-start(bf16[656,128]{1,0:T(8,128)(2,1)S(1)} %get-tuple-element.27.m0), channel_id=1, source_target_pairs={{0,24},{8,0},{16,8},{24,16},{1,25},{9,1},{17,9},{25,17},{2,26},{10... | collective-permute-start | bytes 503816 | tf_op jit(solution)/shard_map/ppermute | solution.py:379
  17.5 5.8 %collective-permute-start.1 = (bf16[656,128]{1,0:T(8,128)(2,1)S(1)}, bf16[656,128]{1,0:T(8,128)(2,1)S(1)}, u32[]{:S(2)}, u32[]{:S(2)}) collective-permute-start(bf16[656,128]{1,0:T(8,128)(2,1)S(1)} %get-tuple-element.27.m0), channel_id=1, source_target_pairs={{0,16},{8,24},{16,0},{24,8},{1,17},{9,25},{17,1},{25,9},{2,18},{10... | collective-permute-start | bytes 503816 | tf_op jit(solution)/shard_map/ppermute | solution.py:379
  18.5 8.9 %collective-permute-start = (bf16[656,128]{1,0:T(8,128)(2,1)S(1)}, bf16[656,128]{1,0:T(8,128)(2,1)S(1)}, u32[]{:S(2)}, u32[]{:S(2)}) collective-permute-start(bf16[656,128]{1,0:T(8,128)(2,1)S(1)} %get-tuple-element.27.m0), channel_id=1, source_target_pairs={{0,8},{8,16},{16,24},{24,0},{1,9},{9,17},{17,25},{25,1},{2,10},{10... | collective-permute-start | bytes 503816 | tf_op jit(solution)/shard_map/ppermute | solution.py:379
  31.6 7.3 %collective-permute-start.6 = (bf16[400,128]{1,0:T(8,128)(2,1)S(1)}, bf16[400,128]{1,0:T(8,128)(2,1)S(1)}, u32[]{:S(2)}, u32[]{:S(2)}) collective-permute-start(bf16[400,128]{1,0:T(8,128)(2,1)S(1)} %get-tuple-element.37), channel_id=1, source_target_pairs={{0,32},{32,64},{64,96},{1,33},{33,65},{65,97},{2,34},{34,66},{66,9... | collective-permute-start | bytes 307208 | tf_op jit(solution)/shard_map/ppermute | solution.py:383
  32.9 5.9 %collective-permute-start.7 = (bf16[400,128]{1,0:T(8,128)(2,1)S(1)}, bf16[400,128]{1,0:T(8,128)(2,1)S(1)}, u32[]{:S(2)}, u32[]{:S(2)}) collective-permute-start(bf16[400,128]{1,0:T(8,128)(2,1)S(1)} %get-tuple-element.38), channel_id=1, source_target_pairs={{0,64},{32,96},{1,65},{33,97},{2,66},{34,98},{3,67},{35,99},{4,68}... | collective-permute-start | bytes 307208 | tf_op jit(solution)/shard_map/ppermute | solution.py:383
  35.8 3.1 %collective-permute-start.8 = (bf16[400,128]{1,0:T(8,128)(2,1)S(1)}, bf16[400,128]{1,0:T(8,128)(2,1)S(1)}, u32[]{:S(2)}, u32[]{:S(2)}) collective-permute-start(bf16[400,128]{1,0:T(8,128)(2,1)S(1)} %get-tuple-element.39), channel_id=1, source_target_pairs={{0,96},{1,97},{2,98},{3,99},{4,100},{5,101},{6,102},{7,103},{8,104... | collective-permute-start | bytes 307208 | tf_op jit(solution)/shard_map/ppermute | solution.py:383
  39.9 2.5 %collective-permute-start.9 = (bf16[128,256]{1,0:T(8,128)(2,1)S(1)}, bf16[128,256]{1,0:T(8,128)(2,1)S(1)}, u32[]{:S(2)}, u32[]{:S(2)}) collective-permute-start(bf16[128,256]{1,0:T(8,128)(2,1)S(1)} %get-tuple-element.41), channel_id=1, source_target_pairs={{0,1},{1,0},{2,3},{3,2},{4,5},{5,4},{6,7},{7,6},{8,9},{9,8},{10,11... | collective-permute-start | bytes 196616 | tf_op jit(solution)/shard_map/ppermute | solution.py:440
  43.5 6.0 %collective-permute-start.12 = (bf16[32,2048]{1,0:T(8,128)(2,1)S(1)}, bf16[32,2048]{1,0:T(8,128)(2,1)S(1)}, u32[]{:S(2)}, u32[]{:S(2)}) collective-permute-start(bf16[32,2048]{1,0:T(8,128)(2,1)S(1)} %get-tuple-element.45), channel_id=1, source_target_pairs={{0,2},{2,4},{4,6},{6,0},{1,3},{3,5},{5,7},{7,1},{8,10},{10,12},{12... | collective-permute-start | bytes 393224 | tf_op jit(solution)/shard_map/ppermute | solution.py:379
  44.8 8.5 %collective-permute-start.13 = (bf16[32,2048]{1,0:T(8,128)(2,1)S(1)}, bf16[32,2048]{1,0:T(8,128)(2,1)S(1)}, u32[]{:S(2)}, u32[]{:S(2)}) collective-permute-start(bf16[32,2048]{1,0:T(8,128)(2,1)S(1)} %get-tuple-element.46), channel_id=1, source_target_pairs={{0,4},{2,6},{4,0},{6,2},{1,5},{3,7},{5,1},{7,3},{8,12},{10,14},{12... | collective-permute-start | bytes 393224 | tf_op jit(solution)/shard_map/ppermute | solution.py:379
  47.2 6.0 %collective-permute-start.14 = (bf16[32,2048]{1,0:T(8,128)(2,1)S(1)}, bf16[32,2048]{1,0:T(8,128)(2,1)S(1)}, u32[]{:S(2)}, u32[]{:S(2)}) collective-permute-start(bf16[32,2048]{1,0:T(8,128)(2,1)S(1)} %get-tuple-element.47), channel_id=1, source_target_pairs={{0,6},{2,0},{4,2},{6,4},{1,7},{3,1},{5,3},{7,5},{8,14},{10,8},{12,... | collective-permute-start | bytes 393224 | tf_op jit(solution)/shard_map/ppermute | solution.py:379
where the time goes:
time: 54.2 us; the launch traced here: 54 us
  starting transfers between devices  21.5 us (40%)
  waiting for transfers between devices  16.8 us (31%)
  Pallas kernels  14.8 us (27%)
  between operations  0.78 us (1%)
    ppermute x6, waiting for transfers between devices, turned(): return lax.ppermute(value, axis, [(i, (i + by) % 4) for i in range(4)])  12.5 us
    ppermute x6, starting transfers between devices, moved(): lax.ppermute(value, axis, [(i, i + by) for i in range(4) if 0 <= i + by <...  9.37 us
    ppermute x6, starting transfers between devices, turned(): return lax.ppermute(value, axis, [(i, (i + by) % 4) for i in range(4)])  9.02 us
    pallas_call x1, Pallas kernels, body(): call(project_kernel, [ANY] * 16, [(tall, BF16), ((Y_ROWS, 128), BF16), (t...  5.33 us
    pallas_call x1, Pallas kernels, body(): call(remote_kernel, [SM] + [VM] * 7, [((Z_ROWS, 128), BF16)] * 3, [pltpu....  4.18 us
    ppermute x6, waiting for transfers between devices, moved(): lax.ppermute(value, axis, [(i, i + by) for i in range(4) if 0 <= i + by <...  3.31 us
    pallas_call x1, Pallas kernels, body(): call(local_kernel, [SM] + [VM] * 7, [(tall, F32), (tall, F32), (tall, F32...  1.72 us
    ppermute x1, starting transfers between devices, body(): taken = lax.ppermute(give, 'c', swap)  1.6 us
  transfers between devices with their start and end apart: 15, of which 7 were waited for; matrix products, arithmetic and copies ran while one was open for 0% of the time, Pallas kernels for 14%

commit v1 on v0

--- a/solution.py
+++ b/solution.py
@@ -139,10 +139,9 @@
 
     lower = subs((ROWS, ROWS)) >= lanes((ROWS, ROWS))
     tri = jnp.where(lower, 1.0, 0.0).astype(BF16)
-    own_run = None
-    for part in split3(log_keep):
-        piece = dot(tri, part)
-        own_run = piece if own_run is None else own_run + piece
+    high, middle, low = split3(log_keep)
+    pair = dot(tri, jnp.concatenate([high, middle], axis=1))
+    own_run = pair[:, 0:128] + pair[:, 128:256] + dot(tri, low)
     extra = jnp.where(lower, jnp.broadcast_to(extra_ref[...], (ROWS, ROWS)), 0.0)
     head_col = jnp.broadcast_to(jnp.sum(extra, axis=-1, keepdims=True), (ROWS, ROWS))
     head_run = head_col[:, 0:128]
@@ -338,13 +337,20 @@
     log_ref[1:2, :] = rows[3:4, :] + rows[4:5, :] + rows[5:6, :] + cum_ref[1:2, :]
 
 
-def out_kernel(at_ref, keep_ref, got_ref, wa, wr, pa, pr, s0, s1, s2, s3, sum_ref):
-    x = at_ref[3]
-    both = jnp.concatenate([keep_ref[...], got_ref[...]], axis=1)
+def own_kernel(keep_ref, wa, wr, own_ref):
+    keep = keep_ref[...]
     for k in range(4):
         cols = slice(512 * k, 512 * k + 512)
-        weight = jnp.concatenate([wa[:, cols], wr[:, cols], pa[:, cols], pr[:, cols]], axis=0)
-        sum_ref[:, cols] = dot(both, weight).astype(BF16)
+        own_ref[:, cols] = dot(keep, jnp.concatenate([wa[:, cols], wr[:, cols]], axis=0))
+
+
+def out_kernel(at_ref, own_ref, got_ref, pa, pr, s0, s1, s2, s3, sum_ref):
+    x = at_ref[3]
+    got = got_ref[...]
+    for k in range(4):
+        cols = slice(512 * k, 512 * k + 512)
+        weight = jnp.concatenate([pa[:, cols], pr[:, cols]], axis=0)
+        sum_ref[:, cols] = (own_ref[:, cols] + dot(got, weight)).astype(BF16)
     for o, out in enumerate((s0, s1, s2, s3)):
         out[...] = sum_ref[pl.ds(32 * lax.rem(x + o, 4), 32), :]
 
@@ -438,9 +444,12 @@
     )
     log_sum = call(log_kernel, [VM] * 2, [((2, ROWS), F32)])(log_total, gate_near)[0]
     taken = lax.ppermute(give, "c", swap)
+    own = call(own_kernel, [VM] * 3, [((128, WIDE), F32)])(
+        keep, attention_output_weight, recurrence_output_weight
+    )[0]
     shares = call(
-        out_kernel, [SM] + [VM] * 6, [((32, WIDE), BF16)] * 4, [pltpu.VMEM((128, WIDE), BF16)]
-    )(at, keep, taken, attention_output_weight, recurrence_output_weight, pa, pr)
+        out_kernel, [SM] + [VM] * 4, [((32, WIDE), BF16)] * 4, [pltpu.VMEM((128, WIDE), BF16)]
+    )(at, own, taken, pa, pr)
     arrived = [shares[0]] + [turned(shares[o], "x", o) for o in (1, 2, 3)]
     mixed = call(add_kernel, [VM] * 4, [((32, WIDE), BF16)])(*arrived)[0]
     return (mixed, log_sum.T)

time: 54.2 us -> 54.1 us (level)
    pallas_call x1 -> x2, Pallas kernels: 1.03 us -> 1.19 us  [the longest x1 0.89 us: body(): call(out_kernel, [SM] + [VM] * 4, [((32, WIDE), BF16)] * 4, [pltpu.VMEM((...]
  transfers between devices with their start and end apart: 15 -> 15, of which waited for: 7 -> 7; matrix products, arithmetic and copies ran while one was open for 0% -> 0% of each run, Pallas kernels for 14% -> 15%
where the time goes in v1:
time: 54.1 us; the launch traced here: 53.9 us
  starting transfers between devices  21.5 us (40%)
  waiting for transfers between devices  16.5 us (30%)
  Pallas kernels  15 us (28%)
  between operations  0.78 us (1%)
    ppermute x6, waiting for transfers between devices, turned(): return lax.ppermute(value, axis, [(i, (i + by) % 4) for i in range(4)])  12.5 us
    ppermute x6, starting transfers between devices, moved(): lax.ppermute(value, axis, [(i, i + by) for i in range(4) if 0 <= i + by <...  9.37 us
    ppermute x6, starting transfers between devices, turned(): return lax.ppermute(value, axis, [(i, (i + by) % 4) for i in range(4)])  9.02 us
    pallas_call x1, Pallas kernels, body(): call(project_kernel, [ANY] * 16, [(tall, BF16), ((Y_ROWS, 128), BF16), (t...  5.35 us
    pallas_call x1, Pallas kernels, body(): call(remote_kernel, [SM] + [VM] * 7, [((Z_ROWS, 128), BF16)] * 3, [pltpu....  4.18 us
    ppermute x6, waiting for transfers between devices, moved(): lax.ppermute(value, axis, [(i, i + by) for i in range(4) if 0 <= i + by <...  3.32 us
    pallas_call x1, Pallas kernels, body(): call(local_kernel, [SM] + [VM] * 7, [(tall, F32), (tall, F32), (tall, F32...  1.72 us
    ppermute x1, starting transfers between devices, body(): taken = lax.ppermute(give, 'c', swap)  1.59 us
  transfers between devices with their start and end apart: 15, of which 7 were waited for; matrix products, arithmetic and copies ran while one was open for 0% of the time, Pallas kernels for 15%

profile of v1, /device:TPU:1, one launch (start us, length us, event | category | flops | bytes accessed | tf_op | source)
XLA Modules:
  0.0 53.9 jit_solution(12950697593672218278)
XLA Ops:
  0.7 5.3 %shard_map.185 = (bf16[256,128]{1,0:T(8,128)(2,1)S(1)}, bf16[656,128]{1,0:T(8,128)(2,1)S(1)}, f32[256,128]{1,0:T(8,128)S(1)}, bf16[256,128]{1,0:T(8,128)(2,1)S(1...) custom-call(bf16[256,2048]{1,0:T(8,128)(2,1)} %x_hbm.1, ...), custom_call_target="tpu_custom_call" | custom-call | tf_op jit(solution)/shard_map/pallas_call | solution.py:404
  6.0 1.5 %collective-permute-start.10 = (bf16[128,2048]{1,0:T(8,128)(2,1)S(1)}, bf16[128,2048]{1,0:T(8,128)(2,1)S(1)}, u32[]{:S(2)}, u32[]{:S(2)}) collective-permute-start(bf16[128,2048]{1,0:T(8,128)(2,1)S(1)} %copy-done), channel_id=1, source_target_pairs={{0,1},{1,0},{2,3},{3,2},{4,5},{5,4},{6,7},{7,6},{8,9},{9,8},{10,11... | collective-permute-start | bytes 1572872 | tf_op jit(solution)/shard_map/ppermute | solution.py:427
  7.5 0.1 collective-permute-start.11
  7.6 1.3 %collective-permute-start.5 = (bf16[256,128]{1,0:T(8,128)(2,1)S(1)}, bf16[256,128]{1,0:T(8,128)(2,1)S(1)}, u32[]{:S(2)}, u32[]{:S(2)}) collective-permute-start(bf16[256,128]{1,0:T(8,128)(2,1)S(1)} %get-tuple-element.26.q_ref), channel_id=1, source_target_pairs={{96,0},{97,1},{98,2},{99,3},{100,4},{101,5},{102,6},{103,7},{104,8... | collective-permute-start | bytes 196616 | tf_op jit(solution)/shard_map/ppermute | solution.py:389
  8.9 1.3 %collective-permute-start.4 = (bf16[256,128]{1,0:T(8,128)(2,1)S(1)}, bf16[256,128]{1,0:T(8,128)(2,1)S(1)}, u32[]{:S(2)}, u32[]{:S(2)}) collective-permute-start(bf16[256,128]{1,0:T(8,128)(2,1)S(1)} %get-tuple-element.26.q_ref), channel_id=1, source_target_pairs={{64,0},{96,32},{65,1},{97,33},{66,2},{98,34},{67,3},{99,35},{68,4}... | collective-permute-start | bytes 196616 | tf_op jit(solution)/shard_map/ppermute | solution.py:389
  10.2 1.3 %collective-permute-start.3 = (bf16[256,128]{1,0:T(8,128)(2,1)S(1)}, bf16[256,128]{1,0:T(8,128)(2,1)S(1)}, u32[]{:S(2)}, u32[]{:S(2)}) collective-permute-start(bf16[256,128]{1,0:T(8,128)(2,1)S(1)} %get-tuple-element.26.q_ref), channel_id=1, source_target_pairs={{32,0},{64,32},{96,64},{33,1},{65,33},{97,65},{34,2},{66,34},{98,6... | collective-permute-start | bytes 196616 | tf_op jit(solution)/shard_map/ppermute | solution.py:389
  11.5 3.3 %collective-permute-done.5.q3 = bf16[256,128]{1,0:T(8,128)(2,1)S(1)} collective-permute-done((bf16[256,128]{1,0:T(8,128)(2,1)S(1)}, bf16[256,128]{1,0:T(8,128)(2,1)S(1)}, u32[]{:S(2)}, u32[]{:S(2)}) %collective-permute-start.5) | collective-permute-done | bytes 65568 | tf_op jit(solution)/shard_map/ppermute | solution.py:389
  14.8 2.7 %collective-permute-start.2 = (bf16[656,128]{1,0:T(8,128)(2,1)S(1)}, bf16[656,128]{1,0:T(8,128)(2,1)S(1)}, u32[]{:S(2)}, u32[]{:S(2)}) collective-permute-start(bf16[656,128]{1,0:T(8,128)(2,1)S(1)} %get-tuple-element.27.m0), channel_id=1, source_target_pairs={{0,24},{8,0},{16,8},{24,16},{1,25},{9,1},{17,9},{25,17},{2,26},{10... | collective-permute-start | bytes 503816 | tf_op jit(solution)/shard_map/ppermute | solution.py:385
  17.5 0.0 collective-permute-done.4.q2
  17.5 1.0 %collective-permute-start.1 = (bf16[656,128]{1,0:T(8,128)(2,1)S(1)}, bf16[656,128]{1,0:T(8,128)(2,1)S(1)}, u32[]{:S(2)}, u32[]{:S(2)}) collective-permute-start(bf16[656,128]{1,0:T(8,128)(2,1)S(1)} %get-tuple-element.27.m0), channel_id=1, source_target_pairs={{0,16},{8,24},{16,0},{24,8},{1,17},{9,25},{17,1},{25,9},{2,18},{10... | collective-permute-start | bytes 503816 | tf_op jit(solution)/shard_map/ppermute | solution.py:385
  18.5 0.4 collective-permute-start
  18.9 0.1 pad_add_fusion.at_ref
  19.0 1.5 %collective-permute-done.2.m3 = bf16[656,128]{1,0:T(8,128)(2,1)S(1)} collective-permute-done((bf16[656,128]{1,0:T(8,128)(2,1)S(1)}, bf16[656,128]{1,0:T(8,128)(2,1)S(1)}, u32[]{:S(2)}, u32[]{:S(2)}) %collective-permute-start.2) | collective-permute-done | bytes 167968 | tf_op jit(solution)/shard_map/ppermute | solution.py:385
  20.5 2.8 %collective-permute-done.1.m2 = bf16[656,128]{1,0:T(8,128)(2,1)S(1)} collective-permute-done((bf16[656,128]{1,0:T(8,128)(2,1)S(1)}, bf16[656,128]{1,0:T(8,128)(2,1)S(1)}, u32[]{:S(2)}, u32[]{:S(2)}) %collective-permute-start.1) | collective-permute-done | bytes 167968 | tf_op jit(solution)/shard_map/ppermute | solution.py:385
  23.3 4.1 %collective-permute-done.m1 = bf16[656,128]{1,0:T(8,128)(2,1)S(1)} collective-permute-done((bf16[656,128]{1,0:T(8,128)(2,1)S(1)}, bf16[656,128]{1,0:T(8,128)(2,1)S(1)}, u32[]{:S(2)}, u32[]{:S(2)}) %collective-permute-start) | collective-permute-done | bytes 167968 | tf_op jit(solution)/shard_map/ppermute | solution.py:385
  27.4 4.2 %shard_map.187 = (bf16[400,128]{1,0:T(8,128)(2,1)S(1)}, bf16[400,128]{1,0:T(8,128)(2,1)S(1)}, bf16[400,128]{1,0:T(8,128)(2,1)S(1)}) custom-call(s32[4]{0:T(128)S(1)} %pad_add_fusion.at_ref, bf16[656,128]{1,0:T(8,128)(2,1)S(1)} %get-tuple-element.27.m0, bf16[656,128]{1,0:T(8,128)(2,1)S(1)} %collective-permute-done.m1, ...), custom_call_target="tpu_custom_call" | custom-call | tf_op jit(solution)/shard_map/pallas_call | solution.py:429
  31.6 1.3 %collective-permute-start.6 = (bf16[400,128]{1,0:T(8,128)(2,1)S(1)}, bf16[400,128]{1,0:T(8,128)(2,1)S(1)}, u32[]{:S(2)}, u32[]{:S(2)}) collective-permute-start(bf16[400,128]{1,0:T(8,128)(2,1)S(1)} %get-tuple-element.37), channel_id=1, source_target_pairs={{0,32},{32,64},{64,96},{1,33},{33,65},{65,97},{2,34},{34,66},{66,9... | collective-permute-start | bytes 307208 | tf_op jit(solution)/shard_map/ppermute | solution.py:389
  32.9 2.9 %collective-permute-start.7 = (bf16[400,128]{1,0:T(8,128)(2,1)S(1)}, bf16[400,128]{1,0:T(8,128)(2,1)S(1)}, u32[]{:S(2)}, u32[]{:S(2)}) collective-permute-start(bf16[400,128]{1,0:T(8,128)(2,1)S(1)} %get-tuple-element.38), channel_id=1, source_target_pairs={{0,64},{32,96},{1,65},{33,97},{2,66},{34,98},{3,67},{35,99},{4,68}... | collective-permute-start | bytes 307208 | tf_op jit(solution)/shard_map/ppermute | solution.py:389
  35.8 1.3 %collective-permute-start.8 = (bf16[400,128]{1,0:T(8,128)(2,1)S(1)}, bf16[400,128]{1,0:T(8,128)(2,1)S(1)}, u32[]{:S(2)}, u32[]{:S(2)}) collective-permute-start(bf16[400,128]{1,0:T(8,128)(2,1)S(1)} %get-tuple-element.39), channel_id=1, source_target_pairs={{0,96},{1,97},{2,98},{3,99},{4,100},{5,101},{6,102},{7,103},{8,104... | collective-permute-start | bytes 307208 | tf_op jit(solution)/shard_map/ppermute | solution.py:389
  37.1 1.7 %shard_map.186 = (f32[256,128]{1,0:T(8,128)S(1)}, f32[256,128]{1,0:T(8,128)S(1)}, f32[256,128]{1,0:T(8,128)S(1)}, f32[8,128]{1,0:T(8,128)S(1)}) custom-call(s32[4]{0:T(128)S(1)} %pad_add_fusion.at_ref, bf16[256,128]{1,0:T(8,128)(2,1)S(1)} %get-tuple-element.26.q_ref, bf16[656,128]{1,0:T(8,128)(2,1)S(1)} %get-tuple-element.27.m0, ...), custom_call_target="tpu_custom_call" | custom-call | tf_op jit(solution)/shard_map/pallas_call | solution.py:434
  38.9 1.1 %shard_map.188 = (bf16[128,256]{1,0:T(8,128)(2,1)S(1)}, bf16[128,256]{1,0:T(8,128)(2,1)S(1)}, f32[256,128]{1,0:T(8,128)S(1)}) custom-call(s32[4]{0:T(128)S(1)} %pad_add_fusion.at_ref, f32[256,128]{1,0:T(8,128)S(1)} %get-tuple-element.30.o_ref, f32[256,128]{1,0:T(8,128)S(1)} %get-tuple-element.31.lse_ref, f32[256,128]{1,0:T(8,128)S(1)} %get-tuple-element.32.rec_ref, ...), custom_call_target="tpu_custom_call" | custom-call | tf_op jit(solution)/shard_map/pallas_call | solution.py:437
  40.0 1.6 %collective-permute-start.9 = (bf16[128,256]{1,0:T(8,128)(2,1)S(1)}, bf16[128,256]{1,0:T(8,128)(2,1)S(1)}, u32[]{:S(2)}, u32[]{:S(2)}) collective-permute-start(bf16[128,256]{1,0:T(8,128)(2,1)S(1)} %get-tuple-element.41), channel_id=1, source_target_pairs={{0,1},{1,0},{2,3},{3,2},{4,5},{5,4},{6,7},{7,6},{8,9},{9,8},{10,11... | collective-permute-start | bytes 196616 | tf_op jit(solution)/shard_map/ppermute | solution.py:446
  41.6 0.3 shard_map.189.own_ref
  41.9 0.6 %collective-permute-done.9.got_ref = bf16[128,256]{1,0:T(8,128)(2,1)S(1)} collective-permute-done((bf16[128,256]{1,0:T(8,128)(2,1)S(1)}, bf16[128,256]{1,0:T(8,128)(2,1)S(1)}, u32[]{:S(2)}, u32[]{:S(2)}) %collective-permute-start.9) | collective-permute-done | bytes 65568 | tf_op jit(solution)/shard_map/ppermute | solution.py:446
  42.5 0.9 %shard_map.190 = (bf16[32,2048]{1,0:T(8,128)(2,1)S(1)}, bf16[32,2048]{1,0:T(8,128)(2,1)S(1)}, bf16[32,2048]{1,0:T(8,128)(2,1)S(1)}, bf16[32,2048]{1,0:T(8,128)(2,1)S(1)}) custom-call(s32[4]{0:T(128)S(1)} %pad_add_fusion.at_ref, f32[128,2048]{1,0:T(8,128)S(1)} %shard_map.189.own_ref, bf16[128,256]{1,0:T(8,128)(2,1)S(1)} %collective-permute-done.9.got_ref, ...), custom_call_target="tpu_custom_call" | custom-call | tf_op jit(solution)/shard_map/pallas_call | solution.py:450
  43.4 1.3 %collective-permute-start.12 = (bf16[32,2048]{1,0:T(8,128)(2,1)S(1)}, bf16[32,2048]{1,0:T(8,128)(2,1)S(1)}, u32[]{:S(2)}, u32[]{:S(2)}) collective-permute-start(bf16[32,2048]{1,0:T(8,128)(2,1)S(1)} %get-tuple-element.45), channel_id=1, source_target_pairs={{0,2},{2,4},{4,6},{6,0},{1,3},{3,5},{5,7},{7,1},{8,10},{10,12},{12... | collective-permute-start | bytes 393224 | tf_op jit(solution)/shard_map/ppermute | solution.py:385
  44.6 2.5 %collective-permute-start.13 = (bf16[32,2048]{1,0:T(8,128)(2,1)S(1)}, bf16[32,2048]{1,0:T(8,128)(2,1)S(1)}, u32[]{:S(2)}, u32[]{:S(2)}) collective-permute-start(bf16[32,2048]{1,0:T(8,128)(2,1)S(1)} %get-tuple-element.46), channel_id=1, source_target_pairs={{0,4},{2,6},{4,0},{6,2},{1,5},{3,7},{5,1},{7,3},{8,12},{10,14},{12... | collective-permute-start | bytes 393224 | tf_op jit(solution)/shard_map/ppermute | solution.py:385
  47.1 1.2 %collective-permute-start.14 = (bf16[32,2048]{1,0:T(8,128)(2,1)S(1)}, bf16[32,2048]{1,0:T(8,128)(2,1)S(1)}, u32[]{:S(2)}, u32[]{:S(2)}) collective-permute-start(bf16[32,2048]{1,0:T(8,128)(2,1)S(1)} %get-tuple-element.47), channel_id=1, source_target_pairs={{0,6},{2,0},{4,2},{6,4},{1,7},{3,1},{5,3},{7,5},{8,14},{10,8},{12,... | collective-permute-start | bytes 393224 | tf_op jit(solution)/shard_map/ppermute | solution.py:385
  48.2 0.8 %shard_map.192 = f32[2,256]{1,0:T(2,128)} custom-call(f32[256,128]{1,0:T(8,128)S(1)} %get-tuple-element.48.total_ref, f32[2,256]{1,0:T(2,128)S(1)} %get-tuple-element.49.cum_ref), custom_call_target="tpu_custom_call" | custom-call | tf_op jit(solution)/shard_map/pallas_call | solution.py:445
  49.0 0.3 collective-permute-done.12.b
  49.3 3.8 %collective-permute-done.13.c = bf16[32,2048]{1,0:T(8,128)(2,1)S(1)} collective-permute-done((bf16[32,2048]{1,0:T(8,128)(2,1)S(1)}, bf16[32,2048]{1,0:T(8,128)(2,1)S(1)}, u32[]{:S(2)}, u32[]{:S(2)}) %collective-permute-start.13) | collective-permute-done | bytes 131104 | tf_op jit(solution)/shard_map/ppermute | solution.py:385
  53.1 0.7 %shard_map.191 = bf16[32,2048]{1,0:T(8,128)(2,1)} custom-call(bf16[32,2048]{1,0:T(8,128)(2,1)S(1)} %get-tuple-element.44.a, bf16[32,2048]{1,0:T(8,128)(2,1)S(1)} %collective-permute-done.12.b, bf16[32,2048]{1,0:T(8,128)(2,1)S(1)} %collective-permute-done.13.c, bf16[32,2048]{1,0:T(8,128)(2,1)S(1)} %collective-permute-done.14.d), custom_call_target="tpu_custom_call" | custom-call | tf_op jit(solution)/shard_map/pallas_call | solution.py:454
  (11 shorter events, 0.0 us)
Async XLA Ops:
  0.6 5.4 %copy-start = (bf16[128,2048]{1,0:T(8,128)(2,1)S(1)}, bf16[128,2048]{1,0:T(8,128)(2,1)}, u32[]{:S(2)}) copy-start(bf16[128,2048]{1,0:T(8,128)(2,1)} %wa.1) | copy-start | bytes 1572868
  0.6 6.8 %copy-start.1 = (bf16[128,2048]{1,0:T(8,128)(2,1)S(1)}, bf16[128,2048]{1,0:T(8,128)(2,1)}, u32[]{:S(2)}) copy-start(bf16[128,2048]{1,0:T(8,128)(2,1)} %wr.1) | copy-start | bytes 1572868
  6.0 36.4 %collective-permute-start.10 = (bf16[128,2048]{1,0:T(8,128)(2,1)S(1)}, bf16[128,2048]{1,0:T(8,128)(2,1)S(1)}, u32[]{:S(2)}, u32[]{:S(2)}) collective-permute-start(bf16[128,2048]{1,0:T(8,128)(2,1)S(1)} %copy-done), channel_id=1, source_target_pairs={{0,1},{1,0},{2,3},{3,2},{4,5},{5,4},{6,7},{7,6},{8,9},{9,8},{10,11... | collective-permute-start | bytes 1572872 | tf_op jit(solution)/shard_map/ppermute | solution.py:427
  7.5 35.0 %collective-permute-start.11 = (bf16[128,2048]{1,0:T(8,128)(2,1)S(1)}, bf16[128,2048]{1,0:T(8,128)(2,1)S(1)}, u32[]{:S(2)}, u32[]{:S(2)}) collective-permute-start(bf16[128,2048]{1,0:T(8,128)(2,1)S(1)} %copy-done.1), channel_id=1, source_target_pairs={{0,1},{1,0},{2,3},{3,2},{4,5},{5,4},{6,7},{7,6},{8,9},{9,8},{10,11... | collective-permute-start | bytes 1572872 | tf_op jit(solution)/shard_map/ppermute | solution.py:428
  7.6 7.2 %collective-permute-start.5 = (bf16[256,128]{1,0:T(8,128)(2,1)S(1)}, bf16[256,128]{1,0:T(8,128)(2,1)S(1)}, u32[]{:S(2)}, u32[]{:S(2)}) collective-permute-start(bf16[256,128]{1,0:T(8,128)(2,1)S(1)} %get-tuple-element.26.q_ref), channel_id=1, source_target_pairs={{96,0},{97,1},{98,2},{99,3},{100,4},{101,5},{102,6},{103,7},{104,8... | collective-permute-start | bytes 196616 | tf_op jit(solution)/shard_map/ppermute | solution.py:389
  8.9 8.6 %collective-permute-start.4 = (bf16[256,128]{1,0:T(8,128)(2,1)S(1)}, bf16[256,128]{1,0:T(8,128)(2,1)S(1)}, u32[]{:S(2)}, u32[]{:S(2)}) collective-permute-start(bf16[256,128]{1,0:T(8,128)(2,1)S(1)} %get-tuple-element.26.q_ref), channel_id=1, source_target_pairs={{64,0},{96,32},{65,1},{97,33},{66,2},{98,34},{67,3},{99,35},{68,4}... | collective-permute-start | bytes 196616 | tf_op jit(solution)/shard_map/ppermute | solution.py:389
  10.2 8.3 %collective-permute-start.3 = (bf16[256,128]{1,0:T(8,128)(2,1)S(1)}, bf16[256,128]{1,0:T(8,128)(2,1)S(1)}, u32[]{:S(2)}, u32[]{:S(2)}) collective-permute-start(bf16[256,128]{1,0:T(8,128)(2,1)S(1)} %get-tuple-element.26.q_ref), channel_id=1, source_target_pairs={{32,0},{64,32},{96,64},{33,1},{65,33},{97,65},{34,2},{66,34},{98,6... | collective-permute-start | bytes 196616 | tf_op jit(solution)/shard_map/ppermute | solution.py:389
  14.8 5.8 %collective-permute-start.2 = (bf16[656,128]{1,0:T(8,128)(2,1)S(1)}, bf16[656,128]{1,0:T(8,128)(2,1)S(1)}, u32[]{:S(2)}, u32[]{:S(2)}) collective-permute-start(bf16[656,128]{1,0:T(8,128)(2,1)S(1)} %get-tuple-element.27.m0), channel_id=1, source_target_pairs={{0,24},{8,0},{16,8},{24,16},{1,25},{9,1},{17,9},{25,17},{2,26},{10... | collective-permute-start | bytes 503816 | tf_op jit(solution)/shard_map/ppermute | solution.py:385
  17.5 5.8 %collective-permute-start.1 = (bf16[656,128]{1,0:T(8,128)(2,1)S(1)}, bf16[656,128]{1,0:T(8,128)(2,1)S(1)}, u32[]{:S(2)}, u32[]{:S(2)}) collective-permute-start(bf16[656,128]{1,0:T(8,128)(2,1)S(1)} %get-tuple-element.27.m0), channel_id=1, source_target_pairs={{0,16},{8,24},{16,0},{24,8},{1,17},{9,25},{17,1},{25,9},{2,18},{10... | collective-permute-start | bytes 503816 | tf_op jit(solution)/shard_map/ppermute | solution.py:385
  18.5 8.9 %collective-permute-start = (bf16[656,128]{1,0:T(8,128)(2,1)S(1)}, bf16[656,128]{1,0:T(8,128)(2,1)S(1)}, u32[]{:S(2)}, u32[]{:S(2)}) collective-permute-start(bf16[656,128]{1,0:T(8,128)(2,1)S(1)} %get-tuple-element.27.m0), channel_id=1, source_target_pairs={{0,8},{8,16},{16,24},{24,0},{1,9},{9,17},{17,25},{25,1},{2,10},{10... | collective-permute-start | bytes 503816 | tf_op jit(solution)/shard_map/ppermute | solution.py:385
  31.6 7.3 %collective-permute-start.6 = (bf16[400,128]{1,0:T(8,128)(2,1)S(1)}, bf16[400,128]{1,0:T(8,128)(2,1)S(1)}, u32[]{:S(2)}, u32[]{:S(2)}) collective-permute-start(bf16[400,128]{1,0:T(8,128)(2,1)S(1)} %get-tuple-element.37), channel_id=1, source_target_pairs={{0,32},{32,64},{64,96},{1,33},{33,65},{65,97},{2,34},{34,66},{66,9... | collective-permute-start | bytes 307208 | tf_op jit(solution)/shard_map/ppermute | solution.py:389
  32.9 6.0 %collective-permute-start.7 = (bf16[400,128]{1,0:T(8,128)(2,1)S(1)}, bf16[400,128]{1,0:T(8,128)(2,1)S(1)}, u32[]{:S(2)}, u32[]{:S(2)}) collective-permute-start(bf16[400,128]{1,0:T(8,128)(2,1)S(1)} %get-tuple-element.38), channel_id=1, source_target_pairs={{0,64},{32,96},{1,65},{33,97},{2,66},{34,98},{3,67},{35,99},{4,68}... | collective-permute-start | bytes 307208 | tf_op jit(solution)/shard_map/ppermute | solution.py:389
  35.8 3.1 %collective-permute-start.8 = (bf16[400,128]{1,0:T(8,128)(2,1)S(1)}, bf16[400,128]{1,0:T(8,128)(2,1)S(1)}, u32[]{:S(2)}, u32[]{:S(2)}) collective-permute-start(bf16[400,128]{1,0:T(8,128)(2,1)S(1)} %get-tuple-element.39), channel_id=1, source_target_pairs={{0,96},{1,97},{2,98},{3,99},{4,100},{5,101},{6,102},{7,103},{8,104... | collective-permute-start | bytes 307208 | tf_op jit(solution)/shard_map/ppermute | solution.py:389
  40.0 2.5 %collective-permute-start.9 = (bf16[128,256]{1,0:T(8,128)(2,1)S(1)}, bf16[128,256]{1,0:T(8,128)(2,1)S(1)}, u32[]{:S(2)}, u32[]{:S(2)}) collective-permute-start(bf16[128,256]{1,0:T(8,128)(2,1)S(1)} %get-tuple-element.41), channel_id=1, source_target_pairs={{0,1},{1,0},{2,3},{3,2},{4,5},{5,4},{6,7},{7,6},{8,9},{9,8},{10,11... | collective-permute-start | bytes 196616 | tf_op jit(solution)/shard_map/ppermute | solution.py:446
  43.4 6.0 %collective-permute-start.12 = (bf16[32,2048]{1,0:T(8,128)(2,1)S(1)}, bf16[32,2048]{1,0:T(8,128)(2,1)S(1)}, u32[]{:S(2)}, u32[]{:S(2)}) collective-permute-start(bf16[32,2048]{1,0:T(8,128)(2,1)S(1)} %get-tuple-element.45), channel_id=1, source_target_pairs={{0,2},{2,4},{4,6},{6,0},{1,3},{3,5},{5,7},{7,1},{8,10},{10,12},{12... | collective-permute-start | bytes 393224 | tf_op jit(solution)/shard_map/ppermute | solution.py:385
  44.6 8.5 %collective-permute-start.13 = (bf16[32,2048]{1,0:T(8,128)(2,1)S(1)}, bf16[32,2048]{1,0:T(8,128)(2,1)S(1)}, u32[]{:S(2)}, u32[]{:S(2)}) collective-permute-start(bf16[32,2048]{1,0:T(8,128)(2,1)S(1)} %get-tuple-element.46), channel_id=1, source_target_pairs={{0,4},{2,6},{4,0},{6,2},{1,5},{3,7},{5,1},{7,3},{8,12},{10,14},{12... | collective-permute-start | bytes 393224 | tf_op jit(solution)/shard_map/ppermute | solution.py:385
  47.1 6.1 %collective-permute-start.14 = (bf16[32,2048]{1,0:T(8,128)(2,1)S(1)}, bf16[32,2048]{1,0:T(8,128)(2,1)S(1)}, u32[]{:S(2)}, u32[]{:S(2)}) collective-permute-start(bf16[32,2048]{1,0:T(8,128)(2,1)S(1)} %get-tuple-element.47), channel_id=1, source_target_pairs={{0,6},{2,0},{4,2},{6,4},{1,7},{3,1},{5,3},{7,5},{8,14},{10,8},{12,... | collective-permute-start | bytes 393224 | tf_op jit(solution)/shard_map/ppermute | solution.py:385
